TPU v7x, 512 devices: a whole 4x4x16 slice. The times are simulated.
512 devices in a mesh: sp: 32 (over z, core), tp: 16 (over y, x).
Axes of the slice: x: 4, y: 4, z: 16, core: 2. Of those that a mesh axis runs over, the one named last changes fastest.
Arguments:
- residual_in: bfloat16 [8192, 2048], P('sp'), may hold values from -3 to 3
- mix_gain: float32 [2048], replicated, may hold values from 0.1 to 1.9
- pool_weight: bfloat16 [512, 2048], P(None, 'tp'), may hold values from -0.5 to 0.5
- pool_scale: float32 [2048], P('tp'), may hold values from 0.1 to 1.9
- ffn_gain: float32 [2048], replicated, may hold values from 0.1 to 1.9
- route_ids: int32 [8192, 2], P('sp'), may hold values from 0 to 31, all different within a row; in each aligned block of 16 rows (0 to 15, 16 to 31, ...) at most 2 rows name the same one
- route_weights: float32 [8192, 2], P('sp'), may hold values from 0.1 to 1
- gate_weight: bfloat16 [32, 2048, 3584], P('sp', None, 'tp'), may hold values from -0.125 to 0.125
- up_weight: bfloat16 [32, 2048, 3584], P('sp', None, 'tp'), may hold values from -0.125 to 0.125
- down_weight: bfloat16 [32, 3584, 2048], P('sp', 'tp'), may hold values from -0.09375 to 0.09375
Outputs:
- layer_out: bfloat16 [8192, 2048], P('sp')
Inputs may be any that keep to these rules, and one draw needn't show every extreme that they name: `route_ids`: each row names 2 different experts; in each aligned block of 16 rows no expert is named by more than 2 rows, and some block has an expert named by exactly 2 rows.
All inputs are finite; a program needn't handle non-finite values.
Results may differ from a plain program's by a relative error of at most 0.0074.
Values may be sent and summed in bfloat16 or wider, within the bound.
No kernel may reach another device: no remote copies, remote signals or barrier semaphores. Data moves between devices by JAX's collectives and lax.ppermute only.
A program may use at most 64 MiB of HBM per device.

v0:
```python
import functools
import math

import jax
import jax.numpy as jnp
import numpy as np
from jax import lax
from jax.experimental import pallas as pl
from jax.experimental.pallas import tpu as pltpu
from jax.sharding import Mesh
from jax.sharding import PartitionSpec as P

GROUPS = 4
SPAN = 16
TOP_K = 2
ROWS = 16
CAP = 2
SP = ("z", "c")
TP = ("y", "x")
ALL = ("z", "c", "y", "x")


EPS = 1e-06
LANES = 128


def from_behind(value, axis, steps):
    count = lax.axis_size(axis)
    first, last = (max(0, -steps), min(count, count - steps))
    return lax.ppermute(value, axis, [(source, source + steps) for source in range(first, last)])


def planes():
    sizes = [lax.axis_size(a) for a in ALL]
    index = np.arange(math.prod(sizes)).reshape(sizes)
    return [
        index[z, c] if c % 2 == 0 else index[z, c].T
        for z in range(sizes[0])
        for c in range(sizes[1])
    ]


def from_quad(value, steps):
    pairs = []
    for plane in planes():
        pairs += list(zip(plane.ravel().tolist(), np.roll(plane, -steps, axis=1).ravel().tolist()))
    return lax.ppermute(value, ALL, pairs)


def from_mate(value, steps):
    sizes = [lax.axis_size(a) for a in ALL]
    index = np.arange(math.prod(sizes)).reshape(sizes)
    pairs = []
    for number, plane in enumerate(planes()):
        owners = index[number // sizes[1], number % sizes[1]]
        pairs += list(zip(np.roll(owners, steps, axis=1).ravel().tolist(), plane.ravel().tolist()))
    return lax.ppermute(value, ALL, pairs)


def exchange(blocks, across=False):
    if across:
        groups = [column for plane in planes() for column in plane.T.tolist()]
    else:
        groups = [plane.ravel().tolist() for plane in planes()]
    return lax.all_to_all(blocks, ALL, 0, 0, tiled=True, axis_index_groups=groups)


def come_back(blocks):
    groups = np.stack([plane.ravel() for plane in planes()], axis=1).tolist()
    return lax.all_to_all(blocks, ALL, 0, 0, tiled=True, axis_index_groups=groups)


def place(t, side, swapped):
    return jnp.where(swapped == 0, t, (t % side) * side + t // side)


def expert_kernel(side, core_ref, x_ref, gain_ref, *refs):
    pieces = (len(refs) - 3) // 3 * 2
    sources, out_ref, normed_ref = (refs[:pieces], refs[pieces], refs[pieces + 1])
    weights, semaphores = (refs[pieces + 2 : -1], refs[-1])
    copies = []
    for i, source in enumerate(sources):
        height = source.shape[0]
        target = weights[i // 2].at[i % 2 * height : (i % 2 + 1) * height]
        copies.append(pltpu.make_async_copy(source, target, semaphores.at[i]))
    for copy in copies:
        copy.start()
    count, rows, lanes = x_ref.shape
    squares = jnp.zeros((rows, lanes), jnp.float32)
    for t in range(count):
        values = x_ref[t].astype(jnp.float32)
        squares = squares + values * values
    inverse = lax.rsqrt(jnp.sum(squares, axis=1, keepdims=True) / (count * lanes) + EPS)
    for t in range(count):
        columns = slice(t * lanes, (t + 1) * lanes)
        values = x_ref[place(t, side, core_ref[0])].astype(jnp.float32)
        normed_ref[:, columns] = (values * inverse * gain_ref[:, columns]).astype(jnp.bfloat16)
    units = weights[0].shape[0] // 3
    contract = (((1,), (1,)), ((), ()))
    normed = normed_ref[...]
    hidden, downs = ([], [])
    for i, ref in enumerate(weights):
        copies[2 * i].wait()
        copies[2 * i + 1].wait()
        gate_rows, up_rows = (ref[:units], ref[units : 2 * units])
        downs.append(ref.at[2 * units :])
        gate = lax.dot_general(normed, gate_rows, contract, preferred_element_type=jnp.float32)
        up = lax.dot_general(normed, up_rows, contract, preferred_element_type=jnp.float32)
        hidden.append((gate * (1.0 / (1.0 + jnp.exp(-gate))) * up).astype(jnp.bfloat16))
    for t in range(0, count, 2):
        total = 0.0
        for part, down in zip(hidden, downs):
            total = total + jnp.dot(
                part,
                down[:, t * lanes : (t + 2) * lanes],
                preferred_element_type=jnp.float32,
            )
        total = total.astype(jnp.bfloat16)
        out_ref[t] = total[:, :lanes]
        out_ref[t + 1] = total[:, lanes:]


SCALARS = pl.BlockSpec(memory_space=pltpu.SMEM)
VECTORS = pl.BlockSpec(memory_space=pltpu.VMEM)
ANYWHERE = pl.BlockSpec(memory_space=pl.ANY)
FAR = pl.BlockSpec(memory_space=pltpu.HBM)


def expert(blocks, core, gain, weights, side):
    count, rows, lanes = blocks.shape
    width = count * lanes
    slices = len(weights) // 2
    height = 2 * weights[0].shape[0]
    units = height // 3
    return pl.pallas_call(
        functools.partial(expert_kernel, side),
        out_shape=jax.ShapeDtypeStruct(blocks.shape, jnp.bfloat16),
        in_specs=[SCALARS, VECTORS, VECTORS] + [ANYWHERE] * len(weights),
        out_specs=VECTORS,
        scratch_shapes=[pltpu.VMEM((rows, width), jnp.bfloat16)]
        + [pltpu.VMEM((height, width), jnp.bfloat16)] * slices
        + [pltpu.SemaphoreType.DMA((len(weights),))],
        compiler_params=pltpu.CompilerParams(vmem_limit_bytes=32 * 2**20),
        cost_estimate=pl.CostEstimate(
            flops=6 * rows * units * width * side,
            bytes_accessed=6 * units * width * side,
            transcendentals=rows * units * side,
        ),
        name="expert",
    )(core, blocks, gain[None], *weights)


def inverse_rms(ref, copies=()):
    rows, width = ref.shape
    squares = jnp.zeros((rows, LANES), jnp.float32)
    for first in range(0, width, LANES):
        if copies and first % (width // len(copies)) == 0:
            copies[first * len(copies) // width].wait()
        values = ref[:, first : first + LANES].astype(jnp.float32)
        squares = squares + values * values
    return lax.rsqrt(jnp.sum(squares, axis=1, keepdims=True) / width + EPS)


def mixer_kernel(
    experts,
    index_ref,
    ids_ref,
    share_ref,
    source_ref,
    rim_ref,
    gain_ref,
    weight_ref,
    scale_ref,
    outgoing_ref,
    plan_ref,
    *refs,
):
    part_refs, (x_ref, after_ref, semaphores) = (refs[:-3], refs[-3:])
    copies = []
    part = source_ref.shape[1] // semaphores.shape[0]
    for i in range(semaphores.shape[0]):
        columns = slice(i * part, (i + 1) * part)
        copies.append(
            pltpu.make_async_copy(source_ref.at[:, columns], x_ref.at[:, columns], semaphores.at[i])
        )
    for copy in copies:
        copy.start()
    group, tp_index, sp_index = (index_ref[0], index_ref[1], index_ref[2])
    rows = x_ref.shape[0]
    span = rim_ref.shape[0]
    group_width, col_count = weight_ref.shape
    columns = pl.ds(pl.multiple_of(group * group_width, group_width), group_width)
    gain = gain_ref[:, columns]

    def normed(ref, inverse):
        return (ref[:, columns].astype(jnp.float32) * inverse * gain).astype(jnp.bfloat16)

    window = jnp.left_shift(2, group)
    here = normed(x_ref, inverse_rms(x_ref, copies))
    row = lax.broadcasted_iota(jnp.int32, (rows, rows), 0)
    col = lax.broadcasted_iota(jnp.int32, (rows, rows), 1)
    band = ((col <= row) & (row - col < window)).astype(jnp.bfloat16)
    sums = jnp.dot(band, here, preferred_element_type=jnp.float32)
    behind = lax.broadcasted_iota(jnp.int32, (rows, span), 0) + span
    behind = behind - lax.broadcasted_iota(jnp.int32, (rows, span), 1)
    sums = sums + jnp.dot(
        (behind < window).astype(jnp.bfloat16), normed(rim_ref, inverse_rms(rim_ref)), preferred_element_type=jnp.float32
    )
    position = sp_index * rows + lax.broadcasted_iota(jnp.int32, (rows, 1), 0)
    divisor = jnp.minimum(position + 1, window).astype(jnp.float32)
    pooled = (sums / divisor - here.astype(jnp.float32)).astype(jnp.bfloat16)
    mixed = jnp.dot(pooled, weight_ref[...], preferred_element_type=jnp.float32) * scale_ref[...]
    own = pl.ds(pl.multiple_of(tp_index * col_count, col_count), col_count)
    stream = x_ref[:, own].astype(jnp.float32)
    after = (stream + mixed.astype(jnp.bfloat16).astype(jnp.float32)).astype(jnp.bfloat16)
    after_ref[...] = after
    height = rows // len(part_refs)
    for step, ref in enumerate(part_refs):
        quarter = (index_ref[3] + step) % len(part_refs)
        ref[...] = after_ref[pl.ds(pl.multiple_of(quarter * height, height), height)]

    ids = ids_ref[...]
    expert_index = lax.broadcasted_iota(jnp.int32, (experts, rows), 0)
    named = [(ids[k : k + 1] == expert_index).astype(jnp.float32) for k in range(TOP_K)]
    earlier = ((row // ROWS == col // ROWS) & (row < col)).astype(jnp.bfloat16)
    before = jnp.dot(
        sum(named).astype(jnp.bfloat16), earlier, preferred_element_type=jnp.float32
    )
    slots = rows // ROWS * CAP
    block = lax.broadcasted_iota(jnp.int32, (1, rows), 1) // ROWS * CAP
    targets = []
    for k in range(TOP_K):
        slot = jnp.sum(before * named[k], axis=0, keepdims=True).astype(jnp.int32)
        targets.append(ids[k : k + 1] * slots + block + slot)
    spare = jnp.zeros((8 - 2 * TOP_K, rows), jnp.float32)
    plan = [target.astype(jnp.float32) for target in targets] + [share_ref[...], spare]
    plan_ref[...] = jnp.concatenate(plan, axis=0).T
    for first in range(0, experts * slots, rows):
        place_here = row + first
        chosen = (place_here == targets[0]) | (place_here == targets[1])
        outgoing_ref[first : first + rows] = jnp.dot(
            chosen.astype(jnp.bfloat16), after, preferred_element_type=jnp.float32
        ).astype(jnp.bfloat16)


def mixer(index, ids, share, x, rim, gain, weight, scale, experts, side):
    rows = x.shape[0]
    col_count = weight.shape[1]
    slots = rows // ROWS * CAP
    return pl.pallas_call(
        functools.partial(mixer_kernel, experts),
        out_shape=(
            jax.ShapeDtypeStruct((experts * slots, col_count), jnp.bfloat16),
            jax.ShapeDtypeStruct((rows, 8), jnp.float32),
            *[jax.ShapeDtypeStruct((rows // side, col_count), jnp.bfloat16)] * side,
        ),
        in_specs=[SCALARS, VECTORS, VECTORS, FAR] + [VECTORS] * 4,
        out_specs=(VECTORS,) * (2 + side),
        scratch_shapes=[
            pltpu.VMEM(x.shape, x.dtype),
            pltpu.VMEM((rows, col_count), jnp.bfloat16),
            pltpu.SemaphoreType.DMA((GROUPS,)),
        ],
        compiler_params=pltpu.CompilerParams(vmem_limit_bytes=16 * 2**20),
        cost_estimate=pl.CostEstimate(
            flops=10**9, bytes_accessed=4 * x.size, transcendentals=rows
        ),
        name="mixer",
    )(index, ids, share, x, rim, gain[None], weight, scale[None])


def combine_kernel(slots, index_ref, returned_ref, plan_ref, parts_ref, out_ref, total_ref):
    side = parts_ref.shape[0]
    rows, _ = total_ref.shape
    quarter = index_ref[4]
    plan = plan_ref[pl.ds(pl.multiple_of(quarter * rows, rows), rows)]
    experts, height = (returned_ref.shape[0], slots // side)
    slot = lax.broadcasted_iota(jnp.int32, (rows, experts * height), 1)
    chosen = []
    for k in range(TOP_K):
        target = plan[:, k : k + 1].astype(jnp.int32)
        target = target // slots * height + target % height
        chosen.append((slot == target).astype(jnp.bfloat16))
    for tile in range(side):
        piece = returned_ref[:, tile * height : (tile + 1) * height].reshape(-1, LANES)
        mix = 0.0
        for k in range(TOP_K):
            picked = jnp.dot(chosen[k], piece, preferred_element_type=jnp.float32)
            mix = mix + plan[:, TOP_K + k : TOP_K + k + 1] * picked
        total_ref[:, tile * LANES : (tile + 1) * LANES] = mix
    for step in range(side):
        column = (quarter + side - step) % side * LANES
        here = pl.ds(pl.multiple_of(column, LANES), LANES)
        total_ref[:, here] = parts_ref[step].astype(jnp.float32) + total_ref[:, here]
    out = total_ref[...].astype(jnp.bfloat16)
    for t in range(out_ref.shape[0]):
        out_ref[t] = out


def combine(index, returned, plan, parts, slots, copies):
    rows, width = (parts.shape[1], parts.shape[0] * LANES)
    return pl.pallas_call(
        functools.partial(combine_kernel, slots),
        out_shape=jax.ShapeDtypeStruct((copies, rows, width), jnp.bfloat16),
        in_specs=[SCALARS] + [VECTORS] * 3,
        out_specs=VECTORS,
        scratch_shapes=[pltpu.VMEM((rows, width), jnp.float32)],
        compiler_params=pltpu.CompilerParams(vmem_limit_bytes=16 * 2**20),
        cost_estimate=pl.CostEstimate(
            flops=4 * returned.size * rows, bytes_accessed=10**6, transcendentals=0
        ),
        name="combine",
    )(index, returned, plan, parts)


def assemble_kernel(side, pieces_ref, out_ref, semaphores):
    count, rows, width = pieces_ref.shape
    copies = []
    for spot in range(count):
        row, quarter = divmod(spot, side)
        target = out_ref.at[quarter * rows : (quarter + 1) * rows, row * width : (row + 1) * width]
        copies.append(pltpu.make_async_copy(pieces_ref.at[spot], target, semaphores.at[spot]))
    for copy in copies:
        copy.start()
    for copy in copies:
        copy.wait()


def assemble(pieces, side):
    count, rows, width = pieces.shape
    return pl.pallas_call(
        functools.partial(assemble_kernel, side),
        out_shape=jax.ShapeDtypeStruct((side * rows, side * width), pieces.dtype),
        in_specs=[VECTORS],
        out_specs=ANYWHERE,
        scratch_shapes=[pltpu.SemaphoreType.DMA((count,))],
        compiler_params=pltpu.CompilerParams(vmem_limit_bytes=4 * 2**20),
        name="assemble",
    )(pieces)


def layer(
    residual_in,
    mix_gain,
    pool_weight,
    pool_scale,
    ffn_gain,
    route_ids,
    route_weights,
    gate_weight,
    up_weight,
    down_weight,
):
    tp_count = lax.axis_size(TP)
    sp_count = lax.axis_size(SP)
    tp_index = lax.axis_index(TP)
    sp_index = lax.axis_index(SP)
    tok_count, width = residual_in.shape
    col_count = pool_weight.shape[1]
    slots = tok_count // ROWS * CAP
    group_index = tp_index * col_count * GROUPS // width

    middle = up_weight.shape[2] // 2
    up_t = up_weight[0].T
    top = jnp.concatenate([gate_weight[0].T, up_t[:middle]], axis=0)
    bottom = jnp.concatenate([up_t[middle:], down_weight[0]], axis=0)
    left_top, right_bottom = (from_quad(top, 1), from_quad(bottom, -1))
    left_bottom, right_top = (from_quad(bottom, 1), from_quad(top, -1))
    rim = from_behind(residual_in[tok_count - SPAN :], SP, 1)

    side = lax.axis_size("x")
    core = lax.axis_index("c").astype(jnp.int32)
    column = lax.axis_index("x")
    place_in_quad = jnp.where(core == 0, column, lax.axis_index("y"))
    index = jnp.stack([group_index, tp_index, sp_index, column, place_in_quad]).astype(jnp.int32)
    core = core.reshape(1)
    outgoing, plan, *parts = mixer(
        index,
        route_ids.T,
        route_weights.T,
        residual_in,
        rim,
        mix_gain,
        pool_weight,
        pool_scale,
        sp_count,
        side,
    )
    outgoing = outgoing.reshape(sp_count, slots, col_count)
    arrived = lax.all_to_all(outgoing, SP, 0, 0, tiled=True)
    far_top, far_bottom = (from_quad(left_top, 1), from_quad(right_bottom, -1))

    parts = [from_mate(part, steps) for steps, part in enumerate(parts)]
    parts = jnp.stack(parts)
    quarter = jnp.moveaxis(arrived.reshape(sp_count, side, -1, col_count), 1, 0)
    quarter = jnp.broadcast_to(quarter[None], (side, *quarter.shape))
    gathered = exchange(quarter.reshape(tp_count, -1, col_count))
    term = expert(gathered, core, ffn_gain, [top, bottom, left_top, left_bottom, right_top, right_bottom, far_top, far_bottom], side)
    summed = exchange(term.reshape(side, side, -1, col_count), across=True)
    expert_out = jnp.sum(summed.astype(jnp.float32), axis=0).astype(jnp.bfloat16)
    expert_out = jnp.moveaxis(expert_out.reshape(side, sp_count, -1, col_count), 0, 1)
    expert_out = expert_out.reshape(sp_count, slots, col_count)
    returned = come_back(expert_out)
    copies = combine(index, returned, plan, parts, slots, tp_count)
    return assemble(exchange(copies), side)


def solution(mesh):
    torus = Mesh(mesh.devices.reshape(-1, 2, 4, mesh.shape["tp"] // 4), ALL)
    return jax.shard_map(
        layer,
        mesh=torus,
        in_specs=(
            P(SP, None),
            P(),
            P(None, TP),
            P(TP),
            P(),
            P(SP, None),
            P(SP, None),
            P(SP, None, TP),
            P(SP, None, TP),
            P(SP, TP, None),
        ),
        out_specs=P(SP, None),
        check_vma=False,
    )
```

profile of v0, /device:TPU:1, one launch (start us, length us, event | category | flops | bytes accessed | tf_op | source)
XLA Modules:
  0.0 167.2 jit_solution(7346752541021945634)
XLA Ops:
  0.0 1.3 fusion
  1.3 0.1 copy-done.7
  1.5 0.1 pad_maximum_fusion.refs_0_
  1.6 4.2 %collective-permute-start.1 = (bf16[336,2048]{1,0:T(8,128)(2,1)S(1)}, bf16[336,2048]{1,0:T(8,128)(2,1)}, u32[]{:S(2)}, u32[]{:S(2)}) collective-permute-start(bf16[336,2048]{1,0:T(8,128)(2,1)S(1)} %pad_maximum_fusion.refs_0_), channel_id=1, source_target_pairs={{0,1},{1,2},{2,3},{3,0},{4,5},{5,6},{6,7},{7,4},{8,9},{9,10},{10,1... | collective-permute-start | bytes 4128776 | tf_op jit(solution)/shard_map/ppermute | solution.py:47
  5.8 0.0 copy-start.2
  5.8 0.0 copy-start.3
  5.8 0.0 copy-start.4
  5.8 0.0 copy-start.5
  5.8 0.0 copy-start.6
  5.8 0.1 pad_maximum_fusion.1.refs_1_
  5.9 3.4 %collective-permute-start.4 = (bf16[336,2048]{1,0:T(8,128)(2,1)S(1)}, bf16[336,2048]{1,0:T(8,128)(2,1)}, u32[]{:S(2)}, u32[]{:S(2)}) collective-permute-start(bf16[336,2048]{1,0:T(8,128)(2,1)S(1)} %pad_maximum_fusion.1.refs_1_), channel_id=1, source_target_pairs={{0,3},{1,0},{2,1},{3,2},{4,7},{5,4},{6,5},{7,6},{8,11},{9,8},{10,9... | collective-permute-start | bytes 4128776 | tf_op jit(solution)/shard_map/ppermute | solution.py:47
  9.3 0.8 slice.9
  10.2 4.6 %collective-permute-start = (bf16[16,2048]{1,0:T(8,128)(2,1)S(1)}, bf16[16,2048]{1,0:T(8,128)(2,1)S(1)}, u32[]{:S(2)}, u32[]{:S(2)}) collective-permute-start(bf16[16,2048]{1,0:T(8,128)(2,1)S(1)} %slice.9), channel_id=1, source_target_pairs={{0,16},{16,32},{32,48},{48,64},{64,80},{80,96},{96,112},{112,128},... | collective-permute-start | bytes 196616 | tf_op jit(solution)/shard_map/ppermute | solution.py:30
  14.8 0.1 stack.38.index_ref
  14.9 3.8 %collective-permute-done.rim_ref = bf16[16,2048]{1,0:T(8,128)(2,1)S(1)} collective-permute-done((bf16[16,2048]{1,0:T(8,128)(2,1)S(1)}, bf16[16,2048]{1,0:T(8,128)(2,1)S(1)}, u32[]{:S(2)}, u32[]{:S(2)}) %collective-permute-start) | collective-permute-done | bytes 65568 | tf_op jit(solution)/shard_map/ppermute | solution.py:30
  18.7 0.0 copy-start.1
  18.7 1.2 copy-done.1
  19.9 2.5 %mixer.1 = (bf16[1024,128]{1,0:T(8,128)(2,1)}, f32[256,8]{1,0:T(8,128)S(1)}, bf16[64,128]{1,0:T(8,128)(2,1)S(1)}, bf16[64,128]{1,0:T(8,128)(2,1)S(1)}, bf16[64,1...) custom-call(s32[5]{0:T(128)S(1)} %stack.38.index_ref, s32[2,256]{1,0:T(2,128)S(1)} %bitcast.40, f32[2,256]{1,0:T(2,128)S(1)} %bitcast.41, ...), custom_call_target="tpu_custom_call" | custom-call | flops 1000000000 | bytes 2097152 | tf_op jit(solution)/shard_map/mixer/pallas_call | solution.py:250
  22.5 14.7 %all-to-all-start = ((bf16[32,32,128]{2,1,0:T(8,128)(2,1)}), bf16[32,32,128]{2,1,0:T(8,128)(2,1)S(1)}, u32[]{:S(2)}, u32[]{:S(2)}) async-start(bf16[32,32,128]{2,1,0:T(8,128)(2,1)} %bitcast.10), calls=%async_computation | async-start | bytes 524288 | tf_op jit(solution)/shard_map/all_to_all | solution.py:390
  37.2 4.6 %collective-permute-start.3 = (bf16[336,2048]{1,0:T(8,128)(2,1)S(1)}, bf16[336,2048]{1,0:T(8,128)(2,1)}, u32[]{:S(2)}, u32[]{:S(2)}) collective-permute-start(bf16[336,2048]{1,0:T(8,128)(2,1)S(1)} %pad_maximum_fusion.refs_0_), channel_id=1, source_target_pairs={{0,3},{1,0},{2,1},{3,2},{4,7},{5,4},{6,5},{7,6},{8,11},{9,8},{10,9... | collective-permute-start | bytes 4128776 | tf_op jit(solution)/shard_map/ppermute | solution.py:47
  41.8 1.9 %collective-permute-start.2 = (bf16[336,2048]{1,0:T(8,128)(2,1)S(1)}, bf16[336,2048]{1,0:T(8,128)(2,1)}, u32[]{:S(2)}, u32[]{:S(2)}) collective-permute-start(bf16[336,2048]{1,0:T(8,128)(2,1)S(1)} %pad_maximum_fusion.1.refs_1_), channel_id=1, source_target_pairs={{0,1},{1,2},{2,3},{3,0},{4,5},{5,6},{6,7},{7,4},{8,9},{9,10},{10,1... | collective-permute-start | bytes 4128776 | tf_op jit(solution)/shard_map/ppermute | solution.py:47
  43.7 0.0 collective-permute-done.1.refs_2_
  43.8 1.9 %collective-permute-start.5 = (bf16[336,2048]{1,0:T(8,128)(2,1)}, bf16[336,2048]{1,0:T(8,128)(2,1)}, u32[]{:S(2)}, u32[]{:S(2)}) collective-permute-start(bf16[336,2048]{1,0:T(8,128)(2,1)} %collective-permute-done.1.refs_2_), channel_id=1, source_target_pairs={{0,1},{1,2},{2,3},{3,0},{4,5},{5,6},{6,7},{7,4},{8,9},{9,10},{10,1... | collective-permute-start | bytes 4128776 | tf_op jit(solution)/shard_map/ppermute | solution.py:47
  45.7 0.0 collective-permute-done.4.refs_5_
  45.7 4.6 %collective-permute-start.6 = (bf16[336,2048]{1,0:T(8,128)(2,1)}, bf16[336,2048]{1,0:T(8,128)(2,1)}, u32[]{:S(2)}, u32[]{:S(2)}) collective-permute-start(bf16[336,2048]{1,0:T(8,128)(2,1)} %collective-permute-done.4.refs_5_), channel_id=1, source_target_pairs={{0,3},{1,0},{2,1},{3,2},{4,7},{5,4},{6,5},{7,6},{8,11},{9,8},{10,9... | collective-permute-start | bytes 4128776 | tf_op jit(solution)/shard_map/ppermute | solution.py:47
  50.3 9.1 %all-to-all-done = bf16[32,32,128]{2,1,0:T(8,128)(2,1)S(1)} async-done(((bf16[32,32,128]{2,1,0:T(8,128)(2,1)}), bf16[32,32,128]{2,1,0:T(8,128)(2,1)S(1)}, u32[]{:S(2)}, u32[]{:S(2)}) %all-to-all-start) | async-done | bytes 262176 | tf_op jit(solution)/shard_map/all_to_all | solution.py:390
  59.5 1.2 broadcast_in_dim.17
  60.6 5.7 %all-to-all-start.1 = ((bf16[16,256,128]{2,1,0:T(8,128)(2,1)}), bf16[16,256,128]{2,1,0:T(8,128)(2,1)}, u32[]{:S(2)}, u32[]{:S(2)}) async-start(bf16[16,256,128]{2,1,0:T(8,128)(2,1)} %bitcast.43), calls=%async_computation.1 | async-start | bytes 2097152 | tf_op jit(solution)/shard_map/all_to_all | solution.py:65
  66.4 0.0 collective-permute-done.3.refs_4_
  66.4 0.0 collective-permute-done.2.refs_3_
  66.4 19.7 %all-to-all-done.1.x_ref = bf16[16,256,128]{2,1,0:T(8,128)(2,1)} async-done(((bf16[16,256,128]{2,1,0:T(8,128)(2,1)}), bf16[16,256,128]{2,1,0:T(8,128)(2,1)}, u32[]{:S(2)}, u32[]{:S(2)}) %all-to-all-start.1) | async-done | bytes 1048608 | tf_op jit(solution)/shard_map/all_to_all | solution.py:65
  86.1 0.0 collective-permute-done.5.refs_6_
  86.1 6.9 %expert.1 = bf16[16,256,128]{2,1,0:T(8,128)(2,1)S(1)} custom-call(s32[1]{0:T(128)} %bitcast.5.core_ref, bf16[16,256,128]{2,1,0:T(8,128)(2,1)} %all-to-all-done.1.x_ref, f32[1,2048]{1,0:T(1,128)S(1)} %bitcast.38, bf16[336,2048]{1,0:T(8,128)(2,1)S(1)} %pad_maximum_fusion.refs_0_, bf16[336,2048]{1,0:T(8,128)(2,1)S(1)} %pad_maximum_fusion.1.refs_1_, ...), custom_call_target="tpu_custom_call" | custom-call | flops 2818572288 | bytes 11010048 | tf_op jit(solution)/shard_map/expert/pallas_call | solution.py:135
  93.0 14.8 %all_to_all.25 = bf16[4,4,256,128]{3,2,1,0:T(8,128)(2,1)S(1)} all-to-all(bf16[4,4,256,128]{3,2,1,0:T(8,128)(2,1)S(1)} %bitcast.37), channel_id=1, replica_groups={{0,4,8,12},{1,5,9,13},{2,6,10,14},{3,7,11,15},{16,17,18,19},{20,21,22,2..., dimensions={0} | all-to-all | bytes 2097152 | tf_op jit(solution)/shard_map/all_to_all | solution.py:65
  107.7 0.2 reduce_sum.12
  107.9 0.7 copy_bitcast_fusion
  108.7 14.7 %all-to-all-start.3 = ((bf16[32,32,128]{2,1,0:T(8,128)(2,1)}), bf16[32,32,128]{2,1,0:T(8,128)(2,1)S(1)}, u32[]{:S(2)}, u32[]{:S(2)}) async-start(bf16[32,32,128]{2,1,0:T(8,128)(2,1)} %copy_bitcast_fusion), calls=%async_computation.3 | async-start | bytes 524288 | tf_op jit(solution)/shard_map/all_to_all | solution.py:70
  123.4 0.7 collective-permute-start.7
  124.0 5.7 %collective-permute-start.8 = (bf16[64,128]{1,0:T(8,128)(2,1)S(1)}, bf16[64,128]{1,0:T(8,128)(2,1)S(1)}, u32[]{:S(2)}, u32[]{:S(2)}) collective-permute-start(bf16[64,128]{1,0:T(8,128)(2,1)S(1)} %get-tuple-element.14), channel_id=1, source_target_pairs={{3,0},{0,1},{1,2},{2,3},{7,4},{4,5},{5,6},{6,7},{11,8},{8,9},{9,10... | collective-permute-start | bytes 49160 | tf_op jit(solution)/shard_map/ppermute | solution.py:57
  129.7 5.2 %collective-permute-start.9 = (bf16[64,128]{1,0:T(8,128)(2,1)S(1)}, bf16[64,128]{1,0:T(8,128)(2,1)S(1)}, u32[]{:S(2)}, u32[]{:S(2)}) collective-permute-start(bf16[64,128]{1,0:T(8,128)(2,1)S(1)} %get-tuple-element.15), channel_id=1, source_target_pairs={{2,0},{3,1},{0,2},{1,3},{6,4},{7,5},{4,6},{5,7},{10,8},{11,9},{8,1... | collective-permute-start | bytes 49160 | tf_op jit(solution)/shard_map/ppermute | solution.py:57
  134.9 5.3 %collective-permute-start.10 = (bf16[64,128]{1,0:T(8,128)(2,1)S(1)}, bf16[64,128]{1,0:T(8,128)(2,1)S(1)}, u32[]{:S(2)}, u32[]{:S(2)}) collective-permute-start(bf16[64,128]{1,0:T(8,128)(2,1)S(1)} %get-tuple-element.16), channel_id=1, source_target_pairs={{1,0},{2,1},{3,2},{0,3},{5,4},{6,5},{7,6},{4,7},{9,8},{10,9},{11,1... | collective-permute-start | bytes 49160 | tf_op jit(solution)/shard_map/ppermute | solution.py:57
  140.2 0.0 collective-permute-done.8
  140.2 0.0 collective-permute-done.9
  140.3 0.8 collective-permute-done.10
  141.1 4.5 %all-to-all-done.3.returned_ref = bf16[32,32,128]{2,1,0:T(8,128)(2,1)S(1)} async-done(((bf16[32,32,128]{2,1,0:T(8,128)(2,1)}), bf16[32,32,128]{2,1,0:T(8,128)(2,1)S(1)}, u32[]{:S(2)}, u32[]{:S(2)}) %all-to-all-start.3) | async-done | bytes 262176 | tf_op jit(solution)/shard_map/all_to_all | solution.py:70
  145.6 0.9 combine.1
  146.6 19.6 %all_to_all.26.pieces_ref = bf16[16,64,512]{2,1,0:T(8,128)(2,1)S(1)} all-to-all(bf16[16,64,512]{2,1,0:T(8,128)(2,1)S(1)} %combine.1), channel_id=1, replica_groups={{0,1,2,3,4,5,6,7,8,9,10,11,12,13,14,15},{16,20,24,28,17,21,25,29,18,22,..., dimensions={0} | all-to-all | bytes 2097152 | tf_op jit(solution)/shard_map/all_to_all | solution.py:65
  166.1 1.1 assemble.1
  (14 shorter events, 0.1 us)
Async XLA Ops:
  0.0 1.5 copy-start.7
  1.5 4.3 %copy-start.8 = (bf16[1,224,2048]{2,1,0:T(8,128)(2,1)S(1)}, bf16[1,224,2048]{2,1,0:T(8,128)(2,1)}, u32[]{:S(2)}) copy-start(bf16[1,224,2048]{2,1,0:T(8,128)(2,1)} %param.19) | copy-start | bytes 2752516
  1.6 42.1 %collective-permute-start.1 = (bf16[336,2048]{1,0:T(8,128)(2,1)S(1)}, bf16[336,2048]{1,0:T(8,128)(2,1)}, u32[]{:S(2)}, u32[]{:S(2)}) collective-permute-start(bf16[336,2048]{1,0:T(8,128)(2,1)S(1)} %pad_maximum_fusion.refs_0_), channel_id=1, source_target_pairs={{0,1},{1,2},{2,3},{3,0},{4,5},{5,6},{6,7},{7,4},{8,9},{9,10},{10,1... | collective-permute-start | bytes 4128776 | tf_op jit(solution)/shard_map/ppermute | solution.py:47
  5.8 12.9 %copy-start.2 = (bf16[512,128]{1,0:T(8,128)(2,1)S(1)}, bf16[512,128]{1,0:T(8,128)(2,1)}, u32[]{:S(2)}) copy-start(bf16[512,128]{1,0:T(8,128)(2,1)} %weight_ref.1) | copy-start | bytes 393220
  5.8 12.9 %copy-start.3 = (f32[2048]{0:T(1024)S(1)}, f32[2048]{0:T(1024)}, u32[]{:S(2)}) copy-start(f32[2048]{0:T(1024)} %param.11) | copy-start | bytes 24580
  5.8 12.9 %copy-start.4 = (s32[256,2]{0,1:T(2,128)S(1)}, s32[256,2]{0,1:T(2,128)}, u32[]{:S(2)}) copy-start(s32[256,2]{0,1:T(2,128)} %param.15) | copy-start | bytes 6148
  5.8 12.9 %copy-start.5 = (f32[256,2]{0,1:T(2,128)S(1)}, f32[256,2]{0,1:T(2,128)}, u32[]{:S(2)}) copy-start(f32[256,2]{0,1:T(2,128)} %param.16) | copy-start | bytes 6148
  5.8 12.9 %copy-start.6 = (f32[128]{0:T(128)S(1)}, f32[128]{0:T(128)}, u32[]{:S(2)}) copy-start(f32[128]{0:T(128)} %param.13) | copy-start | bytes 1540
  5.9 39.7 %collective-permute-start.4 = (bf16[336,2048]{1,0:T(8,128)(2,1)S(1)}, bf16[336,2048]{1,0:T(8,128)(2,1)}, u32[]{:S(2)}, u32[]{:S(2)}) collective-permute-start(bf16[336,2048]{1,0:T(8,128)(2,1)S(1)} %pad_maximum_fusion.1.refs_1_), channel_id=1, source_target_pairs={{0,3},{1,0},{2,1},{3,2},{4,7},{5,4},{6,5},{7,6},{8,11},{9,8},{10,9... | collective-permute-start | bytes 4128776 | tf_op jit(solution)/shard_map/ppermute | solution.py:47
  10.2 8.5 %collective-permute-start = (bf16[16,2048]{1,0:T(8,128)(2,1)S(1)}, bf16[16,2048]{1,0:T(8,128)(2,1)S(1)}, u32[]{:S(2)}, u32[]{:S(2)}) collective-permute-start(bf16[16,2048]{1,0:T(8,128)(2,1)S(1)} %slice.9), channel_id=1, source_target_pairs={{0,16},{16,32},{32,48},{48,64},{64,80},{80,96},{96,112},{112,128},... | collective-permute-start | bytes 196616 | tf_op jit(solution)/shard_map/ppermute | solution.py:30
  18.7 1.2 copy-start.1
  22.5 36.9 %all-to-all-start = ((bf16[32,32,128]{2,1,0:T(8,128)(2,1)}), bf16[32,32,128]{2,1,0:T(8,128)(2,1)S(1)}, u32[]{:S(2)}, u32[]{:S(2)}) async-start(bf16[32,32,128]{2,1,0:T(8,128)(2,1)} %bitcast.10), calls=%async_computation | async-start | bytes 524288 | tf_op jit(solution)/shard_map/all_to_all | solution.py:390
  37.2 29.2 %collective-permute-start.3 = (bf16[336,2048]{1,0:T(8,128)(2,1)S(1)}, bf16[336,2048]{1,0:T(8,128)(2,1)}, u32[]{:S(2)}, u32[]{:S(2)}) collective-permute-start(bf16[336,2048]{1,0:T(8,128)(2,1)S(1)} %pad_maximum_fusion.refs_0_), channel_id=1, source_target_pairs={{0,3},{1,0},{2,1},{3,2},{4,7},{5,4},{6,5},{7,6},{8,11},{9,8},{10,9... | collective-permute-start | bytes 4128776 | tf_op jit(solution)/shard_map/ppermute | solution.py:47
  41.8 24.6 %collective-permute-start.2 = (bf16[336,2048]{1,0:T(8,128)(2,1)S(1)}, bf16[336,2048]{1,0:T(8,128)(2,1)}, u32[]{:S(2)}, u32[]{:S(2)}) collective-permute-start(bf16[336,2048]{1,0:T(8,128)(2,1)S(1)} %pad_maximum_fusion.1.refs_1_), channel_id=1, source_target_pairs={{0,1},{1,2},{2,3},{3,0},{4,5},{5,6},{6,7},{7,4},{8,9},{9,10},{10,1... | collective-permute-start | bytes 4128776 | tf_op jit(solution)/shard_map/ppermute | solution.py:47
  43.8 42.3 %collective-permute-start.5 = (bf16[336,2048]{1,0:T(8,128)(2,1)}, bf16[336,2048]{1,0:T(8,128)(2,1)}, u32[]{:S(2)}, u32[]{:S(2)}) collective-permute-start(bf16[336,2048]{1,0:T(8,128)(2,1)} %collective-permute-done.1.refs_2_), channel_id=1, source_target_pairs={{0,1},{1,2},{2,3},{3,0},{4,5},{5,6},{6,7},{7,4},{8,9},{9,10},{10,1... | collective-permute-start | bytes 4128776 | tf_op jit(solution)/shard_map/ppermute | solution.py:47
  45.7 40.4 %collective-permute-start.6 = (bf16[336,2048]{1,0:T(8,128)(2,1)}, bf16[336,2048]{1,0:T(8,128)(2,1)}, u32[]{:S(2)}, u32[]{:S(2)}) collective-permute-start(bf16[336,2048]{1,0:T(8,128)(2,1)} %collective-permute-done.4.refs_5_), channel_id=1, source_target_pairs={{0,3},{1,0},{2,1},{3,2},{4,7},{5,4},{6,5},{7,6},{8,11},{9,8},{10,9... | collective-permute-start | bytes 4128776 | tf_op jit(solution)/shard_map/ppermute | solution.py:47
  60.6 25.4 %copy-start = (f32[2048]{0:T(1024)S(1)}, f32[2048]{0:T(1024)}, u32[]{:S(2)}) copy-start(f32[2048]{0:T(1024)} %param.14) | copy-start | bytes 24580
  60.6 25.4 %all-to-all-start.1 = ((bf16[16,256,128]{2,1,0:T(8,128)(2,1)}), bf16[16,256,128]{2,1,0:T(8,128)(2,1)}, u32[]{:S(2)}, u32[]{:S(2)}) async-start(bf16[16,256,128]{2,1,0:T(8,128)(2,1)} %bitcast.43), calls=%async_computation.1 | async-start | bytes 2097152 | tf_op jit(solution)/shard_map/all_to_all | solution.py:65
  108.7 36.9 %all-to-all-start.3 = ((bf16[32,32,128]{2,1,0:T(8,128)(2,1)}), bf16[32,32,128]{2,1,0:T(8,128)(2,1)S(1)}, u32[]{:S(2)}, u32[]{:S(2)}) async-start(bf16[32,32,128]{2,1,0:T(8,128)(2,1)} %copy_bitcast_fusion), calls=%async_computation.3 | async-start | bytes 524288 | tf_op jit(solution)/shard_map/all_to_all | solution.py:70
  123.4 16.9 %collective-permute-start.7 = (bf16[64,128]{1,0:T(8,128)(2,1)S(1)}, bf16[64,128]{1,0:T(8,128)(2,1)S(1)}, u32[]{:S(2)}, u32[]{:S(2)}) collective-permute-start(bf16[64,128]{1,0:T(8,128)(2,1)S(1)} %get-tuple-element.13), channel_id=1, source_target_pairs={{0,0},{1,1},{2,2},{3,3},{4,4},{5,5},{6,6},{7,7},{8,8},{9,9},{10,10... | collective-permute-start | bytes 49160 | tf_op jit(solution)/shard_map/ppermute | solution.py:57
  124.0 16.2 %collective-permute-start.8 = (bf16[64,128]{1,0:T(8,128)(2,1)S(1)}, bf16[64,128]{1,0:T(8,128)(2,1)S(1)}, u32[]{:S(2)}, u32[]{:S(2)}) collective-permute-start(bf16[64,128]{1,0:T(8,128)(2,1)S(1)} %get-tuple-element.14), channel_id=1, source_target_pairs={{3,0},{0,1},{1,2},{2,3},{7,4},{4,5},{5,6},{6,7},{11,8},{8,9},{9,10... | collective-permute-start | bytes 49160 | tf_op jit(solution)/shard_map/ppermute | solution.py:57
  129.7 10.5 %collective-permute-start.9 = (bf16[64,128]{1,0:T(8,128)(2,1)S(1)}, bf16[64,128]{1,0:T(8,128)(2,1)S(1)}, u32[]{:S(2)}, u32[]{:S(2)}) collective-permute-start(bf16[64,128]{1,0:T(8,128)(2,1)S(1)} %get-tuple-element.15), channel_id=1, source_target_pairs={{2,0},{3,1},{0,2},{1,3},{6,4},{7,5},{4,6},{5,7},{10,8},{11,9},{8,1... | collective-permute-start | bytes 49160 | tf_op jit(solution)/shard_map/ppermute | solution.py:57
  134.9 6.2 %collective-permute-start.10 = (bf16[64,128]{1,0:T(8,128)(2,1)S(1)}, bf16[64,128]{1,0:T(8,128)(2,1)S(1)}, u32[]{:S(2)}, u32[]{:S(2)}) collective-permute-start(bf16[64,128]{1,0:T(8,128)(2,1)S(1)} %get-tuple-element.16), channel_id=1, source_target_pairs={{1,0},{2,1},{3,2},{0,3},{5,4},{6,5},{7,6},{4,7},{9,8},{10,9},{11,1... | collective-permute-start | bytes 49160 | tf_op jit(solution)/shard_map/ppermute | solution.py:57
where the time goes:
time: 168 us; the launch traced here: 167 us
  starting transfers between devices  77.1 us (46%)
  waiting for transfers between devices  38 us (23%)
  blocking collectives  34.3 us (20%)
  Pallas kernels  11.4 us (7%)
  local copies, waits for them, and re-layouts  5.61 us (3%)
    all_to_all x2, blocking collectives, exchange(): lax.all_to_all(blocks, ALL, 0, 0, tiled=True, axis_index_groups=groups)  34.3 us
    ppermute x6, starting transfers between devices, from_quad(): return lax.ppermute(value, ALL, pairs)  20.6 us
    all_to_all x1, waiting for transfers between devices, exchange(): lax.all_to_all(blocks, ALL, 0, 0, tiled=True, axis_index_groups=groups)  19.7 us
    ppermute x4, starting transfers between devices, from_mate(): return lax.ppermute(value, ALL, pairs)  16.8 us
    all_to_all x1, starting transfers between devices, layer(): arrived = lax.all_to_all(outgoing, SP, 0, 0, tiled=True)  14.7 us
    all_to_all x1, starting transfers between devices, come_back(): lax.all_to_all(blocks, ALL, 0, 0, tiled=True, axis_index_groups=groups)  14.7 us
    all_to_all x1, waiting for transfers between devices, layer(): arrived = lax.all_to_all(outgoing, SP, 0, 0, tiled=True)  9.14 us
    pallas_call x1, Pallas kernels, expert(): pl.pallas_call(functools.partial(expert_kernel, side), out_shape=jax.Shap...  6.88 us
  transfers between devices with their start and end apart: 14, of which 5 were waited for; matrix products, arithmetic and copies ran while one was open for 1% of the time, Pallas kernels for 2%

commit v1 on v0

--- a/solution.py
+++ b/solution.py
@@ -18,7 +18,6 @@
 SP = ("z", "c")
 TP = ("y", "x")
 ALL = ("z", "c", "y", "x")
-
 
 EPS = 1e-06
 LANES = 128
@@ -269,8 +268,9 @@
     )(index, ids, share, x, rim, gain[None], weight, scale[None])
 
 
-def combine_kernel(slots, index_ref, returned_ref, plan_ref, parts_ref, out_ref, total_ref):
-    side = parts_ref.shape[0]
+def combine_kernel(slots, index_ref, returned_ref, plan_ref, *refs):
+    part_refs, out_ref, total_ref = (refs[:-2], refs[-2], refs[-1])
+    side = len(part_refs)
     rows, _ = total_ref.shape
     quarter = index_ref[4]
     plan = plan_ref[pl.ds(pl.multiple_of(quarter * rows, rows), rows)]
@@ -288,21 +288,21 @@
             picked = jnp.dot(chosen[k], piece, preferred_element_type=jnp.float32)
             mix = mix + plan[:, TOP_K + k : TOP_K + k + 1] * picked
         total_ref[:, tile * LANES : (tile + 1) * LANES] = mix
-    for step in range(side):
+    for step, ref in enumerate(part_refs):
         column = (quarter + side - step) % side * LANES
         here = pl.ds(pl.multiple_of(column, LANES), LANES)
-        total_ref[:, here] = parts_ref[step].astype(jnp.float32) + total_ref[:, here]
+        total_ref[:, here] = ref[...].astype(jnp.float32) + total_ref[:, here]
     out = total_ref[...].astype(jnp.bfloat16)
     for t in range(out_ref.shape[0]):
         out_ref[t] = out
 
 
 def combine(index, returned, plan, parts, slots, copies):
-    rows, width = (parts.shape[1], parts.shape[0] * LANES)
+    rows, width = (parts[0].shape[0], len(parts) * LANES)
     return pl.pallas_call(
         functools.partial(combine_kernel, slots),
         out_shape=jax.ShapeDtypeStruct((copies, rows, width), jnp.bfloat16),
-        in_specs=[SCALARS] + [VECTORS] * 3,
+        in_specs=[SCALARS] + [VECTORS] * (2 + len(parts)),
         out_specs=VECTORS,
         scratch_shapes=[pltpu.VMEM((rows, width), jnp.float32)],
         compiler_params=pltpu.CompilerParams(vmem_limit_bytes=16 * 2**20),
@@ -310,7 +310,7 @@
             flops=4 * returned.size * rows, bytes_accessed=10**6, transcendentals=0
         ),
         name="combine",
-    )(index, returned, plan, parts)
+    )(index, returned, plan, *parts)
 
 
 def assemble_kernel(side, pieces_ref, out_ref, semaphores):
@@ -390,8 +390,8 @@
     arrived = lax.all_to_all(outgoing, SP, 0, 0, tiled=True)
     far_top, far_bottom = (from_quad(left_top, 1), from_quad(right_bottom, -1))
 
-    parts = [from_mate(part, steps) for steps, part in enumerate(parts)]
-    parts = jnp.stack(parts)
+    arrived_parts = [from_mate(parts[steps], steps) for steps in (0, 1)]
+    parts = arrived_parts + [from_mate(parts[steps], steps) for steps in (2, 3)]
     quarter = jnp.moveaxis(arrived.reshape(sp_count, side, -1, col_count), 1, 0)
     quarter = jnp.broadcast_to(quarter[None], (side, *quarter.shape))
     gathered = exchange(quarter.reshape(tp_count, -1, col_count))

time: 168 us -> 168 us (level)
  no operation moved by 1% of the time
where the time goes in v1:
time: 168 us; the launch traced here: 167 us
  starting transfers between devices  77.1 us (46%)
  waiting for transfers between devices  38 us (23%)
  blocking collectives  34.3 us (20%)
  Pallas kernels  11.4 us (7%)
  local copies, waits for them, and re-layouts  5.61 us (3%)
    all_to_all x2, blocking collectives, exchange(): lax.all_to_all(blocks, ALL, 0, 0, tiled=True, axis_index_groups=groups)  34.3 us
    ppermute x6, starting transfers between devices, from_quad(): return lax.ppermute(value, ALL, pairs)  20.6 us
    all_to_all x1, waiting for transfers between devices, exchange(): lax.all_to_all(blocks, ALL, 0, 0, tiled=True, axis_index_groups=groups)  19.7 us
    ppermute x4, starting transfers between devices, from_mate(): return lax.ppermute(value, ALL, pairs)  16.8 us
    all_to_all x1, starting transfers between devices, layer(): arrived = lax.all_to_all(outgoing, SP, 0, 0, tiled=True)  14.7 us
    all_to_all x1, starting transfers between devices, come_back(): lax.all_to_all(blocks, ALL, 0, 0, tiled=True, axis_index_groups=groups)  14.7 us
    all_to_all x1, waiting for transfers between devices, layer(): arrived = lax.all_to_all(outgoing, SP, 0, 0, tiled=True)  9.14 us
    pallas_call x1, Pallas kernels, expert(): pl.pallas_call(functools.partial(expert_kernel, side), out_shape=jax.Shap...  6.88 us
  transfers between devices with their start and end apart: 14, of which 5 were waited for; matrix products, arithmetic and copies ran while one was open for 1% of the time, Pallas kernels for 2%

profile of v1, /device:TPU:1, one launch (start us, length us, event | category | flops | bytes accessed | tf_op | source)
XLA Modules:
  0.0 167.2 jit_solution(10236894548287239999)
XLA Ops:
  0.0 1.3 fusion
  1.3 0.1 copy-done.7
  1.5 0.1 pad_maximum_fusion.refs_0_
  1.6 4.2 %collective-permute-start.1 = (bf16[336,2048]{1,0:T(8,128)(2,1)S(1)}, bf16[336,2048]{1,0:T(8,128)(2,1)}, u32[]{:S(2)}, u32[]{:S(2)}) collective-permute-start(bf16[336,2048]{1,0:T(8,128)(2,1)S(1)} %pad_maximum_fusion.refs_0_), channel_id=1, source_target_pairs={{0,1},{1,2},{2,3},{3,0},{4,5},{5,6},{6,7},{7,4},{8,9},{9,10},{10,1... | collective-permute-start | bytes 4128776 | tf_op jit(solution)/shard_map/ppermute | solution.py:46
  5.8 0.0 copy-start.2
  5.8 0.0 copy-start.3
  5.8 0.0 copy-start.4
  5.8 0.0 copy-start.5
  5.8 0.0 copy-start.6
  5.8 0.1 pad_maximum_fusion.1.refs_1_
  5.9 3.4 %collective-permute-start.4 = (bf16[336,2048]{1,0:T(8,128)(2,1)S(1)}, bf16[336,2048]{1,0:T(8,128)(2,1)}, u32[]{:S(2)}, u32[]{:S(2)}) collective-permute-start(bf16[336,2048]{1,0:T(8,128)(2,1)S(1)} %pad_maximum_fusion.1.refs_1_), channel_id=1, source_target_pairs={{0,3},{1,0},{2,1},{3,2},{4,7},{5,4},{6,5},{7,6},{8,11},{9,8},{10,9... | collective-permute-start | bytes 4128776 | tf_op jit(solution)/shard_map/ppermute | solution.py:46
  9.3 0.8 slice.9
  10.2 4.6 %collective-permute-start = (bf16[16,2048]{1,0:T(8,128)(2,1)S(1)}, bf16[16,2048]{1,0:T(8,128)(2,1)S(1)}, u32[]{:S(2)}, u32[]{:S(2)}) collective-permute-start(bf16[16,2048]{1,0:T(8,128)(2,1)S(1)} %slice.9), channel_id=1, source_target_pairs={{0,16},{16,32},{32,48},{48,64},{64,80},{80,96},{96,112},{112,128},... | collective-permute-start | bytes 196616 | tf_op jit(solution)/shard_map/ppermute | solution.py:29
  14.8 0.1 stack.23.index_ref
  14.9 3.8 %collective-permute-done.rim_ref = bf16[16,2048]{1,0:T(8,128)(2,1)S(1)} collective-permute-done((bf16[16,2048]{1,0:T(8,128)(2,1)S(1)}, bf16[16,2048]{1,0:T(8,128)(2,1)S(1)}, u32[]{:S(2)}, u32[]{:S(2)}) %collective-permute-start) | collective-permute-done | bytes 65568 | tf_op jit(solution)/shard_map/ppermute | solution.py:29
  18.7 0.0 copy-start.1
  18.7 1.2 copy-done.1
  19.9 2.5 %mixer.1 = (bf16[1024,128]{1,0:T(8,128)(2,1)}, f32[256,8]{1,0:T(8,128)S(1)}, bf16[64,128]{1,0:T(8,128)(2,1)S(1)}, bf16[64,128]{1,0:T(8,128)(2,1)S(1)}, bf16[64,1...) custom-call(s32[5]{0:T(128)S(1)} %stack.23.index_ref, s32[2,256]{1,0:T(2,128)S(1)} %bitcast.36, f32[2,256]{1,0:T(2,128)S(1)} %bitcast.37, ...), custom_call_target="tpu_custom_call" | custom-call | flops 1000000000 | bytes 2097152 | tf_op jit(solution)/shard_map/mixer/pallas_call | solution.py:249
  22.5 14.7 %all-to-all-start = ((bf16[32,32,128]{2,1,0:T(8,128)(2,1)}), bf16[32,32,128]{2,1,0:T(8,128)(2,1)S(1)}, u32[]{:S(2)}, u32[]{:S(2)}) async-start(bf16[32,32,128]{2,1,0:T(8,128)(2,1)} %bitcast.10), calls=%async_computation | async-start | bytes 524288 | tf_op jit(solution)/shard_map/all_to_all | solution.py:390
  37.2 4.6 %collective-permute-start.3 = (bf16[336,2048]{1,0:T(8,128)(2,1)S(1)}, bf16[336,2048]{1,0:T(8,128)(2,1)}, u32[]{:S(2)}, u32[]{:S(2)}) collective-permute-start(bf16[336,2048]{1,0:T(8,128)(2,1)S(1)} %pad_maximum_fusion.refs_0_), channel_id=1, source_target_pairs={{0,3},{1,0},{2,1},{3,2},{4,7},{5,4},{6,5},{7,6},{8,11},{9,8},{10,9... | collective-permute-start | bytes 4128776 | tf_op jit(solution)/shard_map/ppermute | solution.py:46
  41.8 1.9 %collective-permute-start.2 = (bf16[336,2048]{1,0:T(8,128)(2,1)S(1)}, bf16[336,2048]{1,0:T(8,128)(2,1)}, u32[]{:S(2)}, u32[]{:S(2)}) collective-permute-start(bf16[336,2048]{1,0:T(8,128)(2,1)S(1)} %pad_maximum_fusion.1.refs_1_), channel_id=1, source_target_pairs={{0,1},{1,2},{2,3},{3,0},{4,5},{5,6},{6,7},{7,4},{8,9},{9,10},{10,1... | collective-permute-start | bytes 4128776 | tf_op jit(solution)/shard_map/ppermute | solution.py:46
  43.7 0.0 collective-permute-done.1.refs_2_
  43.8 1.9 %collective-permute-start.5 = (bf16[336,2048]{1,0:T(8,128)(2,1)}, bf16[336,2048]{1,0:T(8,128)(2,1)}, u32[]{:S(2)}, u32[]{:S(2)}) collective-permute-start(bf16[336,2048]{1,0:T(8,128)(2,1)} %collective-permute-done.1.refs_2_), channel_id=1, source_target_pairs={{0,1},{1,2},{2,3},{3,0},{4,5},{5,6},{6,7},{7,4},{8,9},{9,10},{10,1... | collective-permute-start | bytes 4128776 | tf_op jit(solution)/shard_map/ppermute | solution.py:46
  45.7 0.0 collective-permute-done.4.refs_5_
  45.7 4.6 %collective-permute-start.6 = (bf16[336,2048]{1,0:T(8,128)(2,1)}, bf16[336,2048]{1,0:T(8,128)(2,1)}, u32[]{:S(2)}, u32[]{:S(2)}) collective-permute-start(bf16[336,2048]{1,0:T(8,128)(2,1)} %collective-permute-done.4.refs_5_), channel_id=1, source_target_pairs={{0,3},{1,0},{2,1},{3,2},{4,7},{5,4},{6,5},{7,6},{8,11},{9,8},{10,9... | collective-permute-start | bytes 4128776 | tf_op jit(solution)/shard_map/ppermute | solution.py:46
  50.3 9.1 %all-to-all-done = bf16[32,32,128]{2,1,0:T(8,128)(2,1)S(1)} async-done(((bf16[32,32,128]{2,1,0:T(8,128)(2,1)}), bf16[32,32,128]{2,1,0:T(8,128)(2,1)S(1)}, u32[]{:S(2)}, u32[]{:S(2)}) %all-to-all-start) | async-done | bytes 262176 | tf_op jit(solution)/shard_map/all_to_all | solution.py:390
  59.5 1.2 broadcast_in_dim.17
  60.6 5.7 %all-to-all-start.1 = ((bf16[16,256,128]{2,1,0:T(8,128)(2,1)}), bf16[16,256,128]{2,1,0:T(8,128)(2,1)}, u32[]{:S(2)}, u32[]{:S(2)}) async-start(bf16[16,256,128]{2,1,0:T(8,128)(2,1)} %bitcast.39), calls=%async_computation.1 | async-start | bytes 2097152 | tf_op jit(solution)/shard_map/all_to_all | solution.py:64
  66.4 0.0 collective-permute-done.3.refs_4_
  66.4 0.0 collective-permute-done.2.refs_3_
  66.4 19.7 %all-to-all-done.1.x_ref = bf16[16,256,128]{2,1,0:T(8,128)(2,1)} async-done(((bf16[16,256,128]{2,1,0:T(8,128)(2,1)}), bf16[16,256,128]{2,1,0:T(8,128)(2,1)}, u32[]{:S(2)}, u32[]{:S(2)}) %all-to-all-start.1) | async-done | bytes 1048608 | tf_op jit(solution)/shard_map/all_to_all | solution.py:64
  86.1 0.0 collective-permute-done.5.refs_6_
  86.1 6.9 %expert.1 = bf16[16,256,128]{2,1,0:T(8,128)(2,1)S(1)} custom-call(s32[1]{0:T(128)} %bitcast.5.core_ref, bf16[16,256,128]{2,1,0:T(8,128)(2,1)} %all-to-all-done.1.x_ref, f32[1,2048]{1,0:T(1,128)S(1)} %bitcast.34, bf16[336,2048]{1,0:T(8,128)(2,1)S(1)} %pad_maximum_fusion.refs_0_, bf16[336,2048]{1,0:T(8,128)(2,1)S(1)} %pad_maximum_fusion.1.refs_1_, ...), custom_call_target="tpu_custom_call" | custom-call | flops 2818572288 | bytes 11010048 | tf_op jit(solution)/shard_map/expert/pallas_call | solution.py:134
  93.0 14.7 %all_to_all.25 = bf16[4,4,256,128]{3,2,1,0:T(8,128)(2,1)S(1)} all-to-all(bf16[4,4,256,128]{3,2,1,0:T(8,128)(2,1)S(1)} %bitcast.33), channel_id=1, replica_groups={{0,4,8,12},{1,5,9,13},{2,6,10,14},{3,7,11,15},{16,17,18,19},{20,21,22,2..., dimensions={0} | all-to-all | bytes 2097152 | tf_op jit(solution)/shard_map/all_to_all | solution.py:64
  107.7 0.2 reduce_sum.12
  107.9 0.7 copy_bitcast_fusion
  108.7 14.7 %all-to-all-start.3 = ((bf16[32,32,128]{2,1,0:T(8,128)(2,1)}), bf16[32,32,128]{2,1,0:T(8,128)(2,1)S(1)}, u32[]{:S(2)}, u32[]{:S(2)}) async-start(bf16[32,32,128]{2,1,0:T(8,128)(2,1)} %copy_bitcast_fusion), calls=%async_computation.3 | async-start | bytes 524288 | tf_op jit(solution)/shard_map/all_to_all | solution.py:69
  123.4 0.7 collective-permute-start.7
  124.0 5.7 %collective-permute-start.8 = (bf16[64,128]{1,0:T(8,128)(2,1)S(1)}, bf16[64,128]{1,0:T(8,128)(2,1)S(1)}, u32[]{:S(2)}, u32[]{:S(2)}) collective-permute-start(bf16[64,128]{1,0:T(8,128)(2,1)S(1)} %get-tuple-element.14), channel_id=1, source_target_pairs={{3,0},{0,1},{1,2},{2,3},{7,4},{4,5},{5,6},{6,7},{11,8},{8,9},{9,10... | collective-permute-start | bytes 49160 | tf_op jit(solution)/shard_map/ppermute | solution.py:56
  129.7 5.2 %collective-permute-start.9 = (bf16[64,128]{1,0:T(8,128)(2,1)S(1)}, bf16[64,128]{1,0:T(8,128)(2,1)S(1)}, u32[]{:S(2)}, u32[]{:S(2)}) collective-permute-start(bf16[64,128]{1,0:T(8,128)(2,1)S(1)} %get-tuple-element.15), channel_id=1, source_target_pairs={{2,0},{3,1},{0,2},{1,3},{6,4},{7,5},{4,6},{5,7},{10,8},{11,9},{8,1... | collective-permute-start | bytes 49160 | tf_op jit(solution)/shard_map/ppermute | solution.py:56
  134.9 5.3 %collective-permute-start.10 = (bf16[64,128]{1,0:T(8,128)(2,1)S(1)}, bf16[64,128]{1,0:T(8,128)(2,1)S(1)}, u32[]{:S(2)}, u32[]{:S(2)}) collective-permute-start(bf16[64,128]{1,0:T(8,128)(2,1)S(1)} %get-tuple-element.16), channel_id=1, source_target_pairs={{1,0},{2,1},{3,2},{0,3},{5,4},{6,5},{7,6},{4,7},{9,8},{10,9},{11,1... | collective-permute-start | bytes 49160 | tf_op jit(solution)/shard_map/ppermute | solution.py:56
  140.2 0.0 collective-permute-done.7.refs_0_
  140.3 0.0 collective-permute-done.9.refs_2_
  140.3 0.8 collective-permute-done.10.refs_3_
  141.1 4.5 %all-to-all-done.3.returned_ref = bf16[32,32,128]{2,1,0:T(8,128)(2,1)S(1)} async-done(((bf16[32,32,128]{2,1,0:T(8,128)(2,1)}), bf16[32,32,128]{2,1,0:T(8,128)(2,1)S(1)}, u32[]{:S(2)}, u32[]{:S(2)}) %all-to-all-start.3) | async-done | bytes 262176 | tf_op jit(solution)/shard_map/all_to_all | solution.py:69
  145.6 0.9 combine.1
  146.6 19.6 %all_to_all.26.pieces_ref = bf16[16,64,512]{2,1,0:T(8,128)(2,1)S(1)} all-to-all(bf16[16,64,512]{2,1,0:T(8,128)(2,1)S(1)} %combine.1), channel_id=1, replica_groups={{0,1,2,3,4,5,6,7,8,9,10,11,12,13,14,15},{16,20,24,28,17,21,25,29,18,22,..., dimensions={0} | all-to-all | bytes 2097152 | tf_op jit(solution)/shard_map/all_to_all | solution.py:64
  166.1 1.1 assemble.1
  (13 shorter events, 0.1 us)
Async XLA Ops:
  0.0 1.5 copy-start.7
  1.5 4.3 %copy-start.8 = (bf16[1,224,2048]{2,1,0:T(8,128)(2,1)S(1)}, bf16[1,224,2048]{2,1,0:T(8,128)(2,1)}, u32[]{:S(2)}) copy-start(bf16[1,224,2048]{2,1,0:T(8,128)(2,1)} %param.19) | copy-start | bytes 2752516
  1.6 42.1 %collective-permute-start.1 = (bf16[336,2048]{1,0:T(8,128)(2,1)S(1)}, bf16[336,2048]{1,0:T(8,128)(2,1)}, u32[]{:S(2)}, u32[]{:S(2)}) collective-permute-start(bf16[336,2048]{1,0:T(8,128)(2,1)S(1)} %pad_maximum_fusion.refs_0_), channel_id=1, source_target_pairs={{0,1},{1,2},{2,3},{3,0},{4,5},{5,6},{6,7},{7,4},{8,9},{9,10},{10,1... | collective-permute-start | bytes 4128776 | tf_op jit(solution)/shard_map/ppermute | solution.py:46
  5.8 12.9 %copy-start.2 = (bf16[512,128]{1,0:T(8,128)(2,1)S(1)}, bf16[512,128]{1,0:T(8,128)(2,1)}, u32[]{:S(2)}) copy-start(bf16[512,128]{1,0:T(8,128)(2,1)} %weight_ref.1) | copy-start | bytes 393220
  5.8 12.9 %copy-start.3 = (f32[2048]{0:T(1024)S(1)}, f32[2048]{0:T(1024)}, u32[]{:S(2)}) copy-start(f32[2048]{0:T(1024)} %param.11) | copy-start | bytes 24580
  5.8 12.9 %copy-start.4 = (s32[256,2]{0,1:T(2,128)S(1)}, s32[256,2]{0,1:T(2,128)}, u32[]{:S(2)}) copy-start(s32[256,2]{0,1:T(2,128)} %param.15) | copy-start | bytes 6148
  5.8 12.9 %copy-start.5 = (f32[256,2]{0,1:T(2,128)S(1)}, f32[256,2]{0,1:T(2,128)}, u32[]{:S(2)}) copy-start(f32[256,2]{0,1:T(2,128)} %param.16) | copy-start | bytes 6148
  5.8 12.9 %copy-start.6 = (f32[128]{0:T(128)S(1)}, f32[128]{0:T(128)}, u32[]{:S(2)}) copy-start(f32[128]{0:T(128)} %param.13) | copy-start | bytes 1540
  5.9 39.7 %collective-permute-start.4 = (bf16[336,2048]{1,0:T(8,128)(2,1)S(1)}, bf16[336,2048]{1,0:T(8,128)(2,1)}, u32[]{:S(2)}, u32[]{:S(2)}) collective-permute-start(bf16[336,2048]{1,0:T(8,128)(2,1)S(1)} %pad_maximum_fusion.1.refs_1_), channel_id=1, source_target_pairs={{0,3},{1,0},{2,1},{3,2},{4,7},{5,4},{6,5},{7,6},{8,11},{9,8},{10,9... | collective-permute-start | bytes 4128776 | tf_op jit(solution)/shard_map/ppermute | solution.py:46
  10.2 8.5 %collective-permute-start = (bf16[16,2048]{1,0:T(8,128)(2,1)S(1)}, bf16[16,2048]{1,0:T(8,128)(2,1)S(1)}, u32[]{:S(2)}, u32[]{:S(2)}) collective-permute-start(bf16[16,2048]{1,0:T(8,128)(2,1)S(1)} %slice.9), channel_id=1, source_target_pairs={{0,16},{16,32},{32,48},{48,64},{64,80},{80,96},{96,112},{112,128},... | collective-permute-start | bytes 196616 | tf_op jit(solution)/shard_map/ppermute | solution.py:29
  18.7 1.2 copy-start.1
  22.5 36.9 %all-to-all-start = ((bf16[32,32,128]{2,1,0:T(8,128)(2,1)}), bf16[32,32,128]{2,1,0:T(8,128)(2,1)S(1)}, u32[]{:S(2)}, u32[]{:S(2)}) async-start(bf16[32,32,128]{2,1,0:T(8,128)(2,1)} %bitcast.10), calls=%async_computation | async-start | bytes 524288 | tf_op jit(solution)/shard_map/all_to_all | solution.py:390
  37.2 29.2 %collective-permute-start.3 = (bf16[336,2048]{1,0:T(8,128)(2,1)S(1)}, bf16[336,2048]{1,0:T(8,128)(2,1)}, u32[]{:S(2)}, u32[]{:S(2)}) collective-permute-start(bf16[336,2048]{1,0:T(8,128)(2,1)S(1)} %pad_maximum_fusion.refs_0_), channel_id=1, source_target_pairs={{0,3},{1,0},{2,1},{3,2},{4,7},{5,4},{6,5},{7,6},{8,11},{9,8},{10,9... | collective-permute-start | bytes 4128776 | tf_op jit(solution)/shard_map/ppermute | solution.py:46
  41.8 24.6 %collective-permute-start.2 = (bf16[336,2048]{1,0:T(8,128)(2,1)S(1)}, bf16[336,2048]{1,0:T(8,128)(2,1)}, u32[]{:S(2)}, u32[]{:S(2)}) collective-permute-start(bf16[336,2048]{1,0:T(8,128)(2,1)S(1)} %pad_maximum_fusion.1.refs_1_), channel_id=1, source_target_pairs={{0,1},{1,2},{2,3},{3,0},{4,5},{5,6},{6,7},{7,4},{8,9},{9,10},{10,1... | collective-permute-start | bytes 4128776 | tf_op jit(solution)/shard_map/ppermute | solution.py:46
  43.8 42.3 %collective-permute-start.5 = (bf16[336,2048]{1,0:T(8,128)(2,1)}, bf16[336,2048]{1,0:T(8,128)(2,1)}, u32[]{:S(2)}, u32[]{:S(2)}) collective-permute-start(bf16[336,2048]{1,0:T(8,128)(2,1)} %collective-permute-done.1.refs_2_), channel_id=1, source_target_pairs={{0,1},{1,2},{2,3},{3,0},{4,5},{5,6},{6,7},{7,4},{8,9},{9,10},{10,1... | collective-permute-start | bytes 4128776 | tf_op jit(solution)/shard_map/ppermute | solution.py:46
  45.7 40.4 %collective-permute-start.6 = (bf16[336,2048]{1,0:T(8,128)(2,1)}, bf16[336,2048]{1,0:T(8,128)(2,1)}, u32[]{:S(2)}, u32[]{:S(2)}) collective-permute-start(bf16[336,2048]{1,0:T(8,128)(2,1)} %collective-permute-done.4.refs_5_), channel_id=1, source_target_pairs={{0,3},{1,0},{2,1},{3,2},{4,7},{5,4},{6,5},{7,6},{8,11},{9,8},{10,9... | collective-permute-start | bytes 4128776 | tf_op jit(solution)/shard_map/ppermute | solution.py:46
  60.6 25.4 %copy-start = (f32[2048]{0:T(1024)S(1)}, f32[2048]{0:T(1024)}, u32[]{:S(2)}) copy-start(f32[2048]{0:T(1024)} %param.14) | copy-start | bytes 24580
  60.6 25.4 %all-to-all-start.1 = ((bf16[16,256,128]{2,1,0:T(8,128)(2,1)}), bf16[16,256,128]{2,1,0:T(8,128)(2,1)}, u32[]{:S(2)}, u32[]{:S(2)}) async-start(bf16[16,256,128]{2,1,0:T(8,128)(2,1)} %bitcast.39), calls=%async_computation.1 | async-start | bytes 2097152 | tf_op jit(solution)/shard_map/all_to_all | solution.py:64
  108.7 36.9 %all-to-all-start.3 = ((bf16[32,32,128]{2,1,0:T(8,128)(2,1)}), bf16[32,32,128]{2,1,0:T(8,128)(2,1)S(1)}, u32[]{:S(2)}, u32[]{:S(2)}) async-start(bf16[32,32,128]{2,1,0:T(8,128)(2,1)} %copy_bitcast_fusion), calls=%async_computation.3 | async-start | bytes 524288 | tf_op jit(solution)/shard_map/all_to_all | solution.py:69
  123.4 16.9 %collective-permute-start.7 = (bf16[64,128]{1,0:T(8,128)(2,1)S(1)}, bf16[64,128]{1,0:T(8,128)(2,1)S(1)}, u32[]{:S(2)}, u32[]{:S(2)}) collective-permute-start(bf16[64,128]{1,0:T(8,128)(2,1)S(1)} %get-tuple-element.13), channel_id=1, source_target_pairs={{0,0},{1,1},{2,2},{3,3},{4,4},{5,5},{6,6},{7,7},{8,8},{9,9},{10,10... | collective-permute-start | bytes 49160 | tf_op jit(solution)/shard_map/ppermute | solution.py:56
  124.0 16.2 %collective-permute-start.8 = (bf16[64,128]{1,0:T(8,128)(2,1)S(1)}, bf16[64,128]{1,0:T(8,128)(2,1)S(1)}, u32[]{:S(2)}, u32[]{:S(2)}) collective-permute-start(bf16[64,128]{1,0:T(8,128)(2,1)S(1)} %get-tuple-element.14), channel_id=1, source_target_pairs={{3,0},{0,1},{1,2},{2,3},{7,4},{4,5},{5,6},{6,7},{11,8},{8,9},{9,10... | collective-permute-start | bytes 49160 | tf_op jit(solution)/shard_map/ppermute | solution.py:56
  129.7 10.5 %collective-permute-start.9 = (bf16[64,128]{1,0:T(8,128)(2,1)S(1)}, bf16[64,128]{1,0:T(8,128)(2,1)S(1)}, u32[]{:S(2)}, u32[]{:S(2)}) collective-permute-start(bf16[64,128]{1,0:T(8,128)(2,1)S(1)} %get-tuple-element.15), channel_id=1, source_target_pairs={{2,0},{3,1},{0,2},{1,3},{6,4},{7,5},{4,6},{5,7},{10,8},{11,9},{8,1... | collective-permute-start | bytes 49160 | tf_op jit(solution)/shard_map/ppermute | solution.py:56
  134.9 6.2 %collective-permute-start.10 = (bf16[64,128]{1,0:T(8,128)(2,1)S(1)}, bf16[64,128]{1,0:T(8,128)(2,1)S(1)}, u32[]{:S(2)}, u32[]{:S(2)}) collective-permute-start(bf16[64,128]{1,0:T(8,128)(2,1)S(1)} %get-tuple-element.16), channel_id=1, source_target_pairs={{1,0},{2,1},{3,2},{0,3},{5,4},{6,5},{7,6},{4,7},{9,8},{10,9},{11,1... | collective-permute-start | bytes 49160 | tf_op jit(solution)/shard_map/ppermute | solution.py:56
